TPU v7x, 32 devices: a whole 2x2x4 slice. The times are simulated.
32 devices in a mesh: ep: 8 (over z, x), tp: 4 (over y, core).
Axes of the slice: x: 2, y: 2, z: 4, core: 2. Of those that a mesh axis runs over, the one named last changes fastest.
Arguments:
- tokens: bfloat16 [5120, 2048], P(('ep', 'tp')), may hold values from -6 to 6
- expert_ids: int32 [5120, 2], P(('ep', 'tp')), may hold values from 0 to 7, all different within a row; in each aligned block of 160 rows (0 to 159, 160 to 319, ...) at most 60 rows name the same one
- group_weight: float32 [5120], P(('ep', 'tp')), may hold values from 0.3 to 1
- expert_share: float32 [5120, 2], P(('ep', 'tp')), may hold values from 0.05 to 1
- gate_w: bfloat16 [8, 512, 2048], P('ep', 'tp'), may hold values from -0.125 to 0.125
- up_w: bfloat16 [8, 512, 2048], P('ep', 'tp'), may hold values from -0.125 to 0.125
- down_w: bfloat16 [8, 512, 2048], P('ep', 'tp'), may hold values from -0.25 to 0.25
- out_gain: float32 [2048], replicated, may hold values from 0.1 to 1.9
- out_shift: float32 [2048], replicated, may hold values from -3 to 3
Outputs:
- layer_out: bfloat16 [5120, 2048], P(('ep', 'tp'))
Inputs may be any that keep to these rules, and one draw needn't show every extreme that they name: `expert_ids`: the 2 ids of a token differ. Among the rows of one device no id is named more than 60 times, and in some device's rows some id is named exactly 60 times.
All inputs are finite; a program needn't handle non-finite values.
Results may differ from a plain program's by a relative error of at most 0.0021.
Values may be sent and summed in bfloat16 or wider, within the bound.
A program may use at most 64 MiB of HBM per device.

v0:
```python
import jax
import jax.numpy as jnp
from jax import lax
from jax.sharding import PartitionSpec as P

TOP = 2


residual_scale = 2.0**0.5
norm_eps = 1e-05


def layer_norm(values, gain, shift):
    center = values - jnp.mean(values, axis=-1, keepdims=True)
    variance = jnp.mean(center * center, axis=-1, keepdims=True)
    return (center * lax.rsqrt(variance + norm_eps) * gain + shift).astype(jnp.bfloat16)


def body(tokens, expert_ids, group_weight, expert_share, gate_w, up_w, down_w, out_gain, out_shift):
    tok_count, model_width = tokens.shape
    ep_size = lax.axis_size("ep")
    local_count = gate_w.shape[0]
    experts_all = ep_size * local_count
    capacity = 3 * tok_count * TOP // (2 * experts_all)
    flat_ids = expert_ids.reshape(-1)
    onehot = (flat_ids[:, None] == jnp.arange(experts_all, dtype=jnp.int32)[None, :]).astype(
        jnp.int32
    )
    earlier = jnp.cumsum(onehot, axis=0) - onehot
    slot_index = jnp.sum(earlier * onehot, axis=1)
    dest_index = flat_ids * capacity + slot_index
    copies = jnp.repeat(tokens, TOP, axis=0)
    send_buf = (
        jnp.zeros((experts_all * capacity, model_width), tokens.dtype).at[dest_index].set(copies)
    )
    send_buf = send_buf.reshape(ep_size, local_count * capacity, model_width)
    received = lax.all_to_all(send_buf, "ep", split_axis=0, concat_axis=0, tiled=True)
    expert_rows = received.reshape(ep_size, local_count, capacity, model_width)
    expert_rows = expert_rows.transpose(1, 0, 2, 3).reshape(
        local_count, ep_size * capacity, model_width
    )
    gate_piece = lax.all_gather(gate_w, "tp", axis=1, tiled=True)
    up_piece = lax.all_gather(up_w, "tp", axis=1, tiled=True)
    down_piece = lax.all_gather(down_w, "tp", axis=1, tiled=True)
    gate_act = jnp.einsum(
        "lrd,lfd->lrf", expert_rows, gate_piece, preferred_element_type=jnp.float32
    )
    up_act = jnp.einsum("lrd,lfd->lrf", expert_rows, up_piece, preferred_element_type=jnp.float32)
    hidden = (jax.nn.silu(gate_act) * up_act).astype(jnp.bfloat16)
    expert_out = jnp.einsum("lrf,lfd->lrd", hidden, down_piece, preferred_element_type=jnp.float32)
    results = expert_out.astype(jnp.bfloat16).reshape(local_count, ep_size, capacity, model_width)
    results = results.transpose(1, 0, 2, 3).reshape(ep_size, local_count * capacity, model_width)
    returned = lax.all_to_all(results, "ep", split_axis=0, concat_axis=0, tiled=True)
    returned = returned.reshape(experts_all * capacity, model_width)
    picked = returned[dest_index].reshape(tok_count, TOP, model_width)
    share_norm = expert_share / jnp.sum(expert_share, axis=1, keepdims=True)
    route_weight = group_weight[:, None] * share_norm
    mixture = jnp.sum(route_weight[:, :, None] * picked.astype(jnp.float32), axis=1)
    residual = residual_scale * tokens.astype(jnp.float32) + mixture
    return layer_norm(residual, out_gain, out_shift)


def solution(mesh):
    placed = (
        P(("ep", "tp"), None),
        P(("ep", "tp"), None),
        P(("ep", "tp")),
        P(("ep", "tp"), None),
        P("ep", "tp", None),
        P("ep", "tp", None),
        P("ep", "tp", None),
        P(),
        P(),
    )
    return jax.shard_map(
        body, mesh=mesh, in_specs=placed, out_specs=P(("ep", "tp"), None), check_vma=False
    )
```

profile of v0, /device:TPU:0, one launch (start us, length us, event | category | flops | bytes accessed | tf_op | source)
XLA Modules:
  0.0 165.9 jit_solution(13100133334638237621)
XLA Ops:
  6.5 0.7 all-gather.4.cloned.1.call-update
  7.3 0.7 all-gather.6.cloned.1.call-update
  8.0 0.8 copy.13
  8.8 0.1 eq.22
  9.0 0.9 reduce-window.6
  9.8 0.2 slice_reduce_fusion
  10.1 0.7 broadcast_multiply_fusion
  10.8 0.1 copy.12
  10.9 0.1 mul.76
  11.0 1.9 %broadcast_in_dim.5 = bf16[160,2,2048]{2,1,0:T(2,128)(2,1)S(1)} broadcast(bf16[160,2048]{1,0:T(8,128)(2,1)} %param.9), dimensions={0,2} | broadcast | bytes 1966080 | tf_op jit(solution)/shard_map/broadcast_in_dim | solution.py:32
  12.9 0.5 reshape.122
  13.5 0.1 add_bitcast_fusion
  13.6 3.1 %scatter_custom_fusion = bf16[480,2048]{1,0:T(8,128)(2,1)S(1)} fusion(s32[320]{0:T(512)S(1)} %fusion.19, bf16[320,2048]{1,0:T(8,128)(2,1)S(1)} %reshape.122, bf16[]{:T(256)} %constant.8.clone.1), kind=kCustom, calls=%fused_computation.14 | custom fusion | bytes 1966082 | tf_op jit(solution)/shard_map/scatter | solution.py:34
  16.7 1.6 reshape.102
  18.3 7.3 %all-to-all-start = ((bf16[8,60,2048]{2,1,0:T(8,128)(2,1)}), bf16[8,60,2048]{2,1,0:T(8,128)(2,1)S(1)}, u32[]{:S(2)}, u32[]{:S(2)}) async-start(bf16[8,60,2048]{2,1,0:T(8,128)(2,1)} %reshape.102), calls=%async_computation | async-start | bytes 4194304 | tf_op jit(solution)/shard_map/all_to_all | solution.py:37
  25.6 0.7 all-gather.8.cloned.1.call-update
  26.3 47.5 %all-to-all-done = bf16[8,60,2048]{2,1,0:T(8,128)(2,1)S(1)} async-done(((bf16[8,60,2048]{2,1,0:T(8,128)(2,1)}), bf16[8,60,2048]{2,1,0:T(8,128)(2,1)S(1)}, u32[]{:S(2)}, u32[]{:S(2)}) %all-to-all-start) | async-done | bytes 1966112 | tf_op jit(solution)/shard_map/all_to_all | solution.py:37
  73.8 1.5 reshape.103
  75.3 3.6 %fusion.3 = f32[480,512]{1,0:T(8,128)S(1)} fusion(bf16[480,2048]{1,0:T(8,128)(2,1)} %reshape.103, bf16[1,512,2048]{2,1,0:T(8,128)(2,1)} %all-gather.4.cloned.1.call-done), kind=kOutput, calls=%fused_computation.7 | convolution fusion | flops 1006632960 | bytes 5046272 | tf_op jit(solution)/shard_map/lrd,lfd->lrf/dot_general | solution.py:45
  78.9 3.7 %all-gather.8.cloned.1.call-done = bf16[1,512,2048]{2,1,0:T(8,128)(2,1)} async-done(((bf16[1,128,2048]{2,1,0:T(8,128)(2,1)}), bf16[1,512,2048]{2,1,0:T(8,128)(2,1)}) %all-gather.8.cloned.1.call-update) | async-done | bytes 2097168 | tf_op jit(solution)/shard_map/all_gather | solution.py:44
  82.6 5.9 %convolution_convert_fusion = bf16[480,2048]{1,0:T(8,128)(2,1)} fusion(bf16[1,512,2048]{2,1,0:T(8,128)(2,1)} %all-gather.8.cloned.1.call-done, bf16[480,2048]{1,0:T(8,128)(2,1)S(1)} %copy-done.1, bf16[1,512,2048]{2,1,0:T(8,128)(2,1)} %all-gather.6.cloned.1.call-done, f32[480,512]{1,0:T(8,128)S(1)} %fusion.3), kind=kOutput, calls=%fused_computation.2 | convolution fusion | flops 2015723520 | bytes 9109504 | tf_op jit(solution)/shard_map/lrf,lfd->lrd/dot_general | solution.py:50
  88.4 2.7 %reshape_transpose_reshape.4 = bf16[8,60,2048]{2,1,0:T(8,128)(2,1)} reshape(bf16[480,2048]{1,0:T(8,128)(2,1)} %convolution_convert_fusion) | data formatting | bytes 3932160 | tf_op jit(solution)/shard_map/reshape;transpose;reshape | solution.py:52
  91.2 5.6 %all-to-all-start.1 = ((bf16[8,60,2048]{2,1,0:T(8,128)(2,1)}), bf16[8,60,2048]{2,1,0:T(8,128)(2,1)}, u32[]{:S(2)}, u32[]{:S(2)}) async-start(bf16[8,60,2048]{2,1,0:T(8,128)(2,1)} %reshape_transpose_reshape.4), calls=%async_computation.1 | async-start | bytes 4194304 | tf_op jit(solution)/shard_map/all_to_all | solution.py:53
  96.8 0.1 copy.11
  97.0 48.6 %all-to-all-done.1 = bf16[8,60,2048]{2,1,0:T(8,128)(2,1)} async-done(((bf16[8,60,2048]{2,1,0:T(8,128)(2,1)}), bf16[8,60,2048]{2,1,0:T(8,128)(2,1)}, u32[]{:S(2)}, u32[]{:S(2)}) %all-to-all-start.1) | async-done | bytes 1966112 | tf_op jit(solution)/shard_map/all_to_all | solution.py:53
  145.5 1.7 %reshape.107 = bf16[480,2048]{1,0:T(8,128)(2,1)S(1)} reshape(bf16[8,60,2048]{2,1,0:T(8,128)(2,1)} %all-to-all-done.1) | data formatting | bytes 3932160 | tf_op jit(solution)/shard_map/reshape | solution.py:54
  147.3 3.0 %gather_fusion = bf16[320,2048]{1,0:T(8,128)(2,1)} fusion(bf16[480,2048]{1,0:T(8,128)(2,1)S(1)} %reshape.107, s32[1024]{0:T(1024)S(1)} %pad_clamp_fusion), kind=kCustom, calls=%fused_computation | custom fusion | bytes 2622720 | tf_op jit(solution)/shard_map/gather | solution.py:55
  150.3 3.1 %reshape.109 = f32[160,2,2048]{2,1,0:T(2,128)S(1)} reshape(bf16[320,2048]{1,0:T(8,128)(2,1)} %gather_fusion) | data formatting | bytes 3932160 | tf_op jit(solution)/shard_map/convert_element_type | solution.py:58
  153.4 4.1 %multiply_reduce_fusion = f32[160,2048]{1,0:T(8,128)S(1)} fusion(f32[160,2,2048]{2,1,0:T(2,128)S(1)} %reshape.109, f32[160,2]{1,0:T(8,128)S(1)} %copy.11), kind=kLoop, calls=%fused_computation.3 | loop fusion | flops 983040 | bytes 3933440 | tf_op jit(solution)/shard_map/reduce_sum | solution.py:58
  157.5 0.3 fusion.16
  157.8 0.4 multiply_reduce_fusion.1
  158.2 1.2 add_convert_fusion
  (27 shorter events, 0.3 us)
Async XLA Ops:
  6.5 68.7 %all-gather.4.cloned.1.call-start = ((), (), s32[]{:S(2)}) async-start(), calls=%async_computation.2 | async-start | bytes 2621440 | tf_op jit(solution)/shard_map/all_gather | solution.py:42
  7.3 71.6 %all-gather.6.cloned.1.call-start = ((), (), s32[]{:S(2)}) async-start(), calls=%async_computation.3 | async-start | bytes 2621440 | tf_op jit(solution)/shard_map/all_gather | solution.py:43
  18.3 55.5 %all-to-all-start = ((bf16[8,60,2048]{2,1,0:T(8,128)(2,1)}), bf16[8,60,2048]{2,1,0:T(8,128)(2,1)S(1)}, u32[]{:S(2)}, u32[]{:S(2)}) async-start(bf16[8,60,2048]{2,1,0:T(8,128)(2,1)} %reshape.102), calls=%async_computation | async-start | bytes 4194304 | tf_op jit(solution)/shard_map/all_to_all | solution.py:37
  25.6 57.0 %all-gather.8.cloned.1.call-start = ((), (), s32[]{:S(2)}) async-start(), calls=%async_computation.4 | async-start | bytes 2621440 | tf_op jit(solution)/shard_map/all_gather | solution.py:44
  75.3 7.3 %copy-start.1 = (bf16[480,2048]{1,0:T(8,128)(2,1)S(1)}, bf16[480,2048]{1,0:T(8,128)(2,1)}, u32[]{:S(2)}) copy-start(bf16[480,2048]{1,0:T(8,128)(2,1)} %reshape.103) | copy-start | bytes 5898244
  91.1 5.6 %copy-start.4 = (f32[160,2]{0,1:T(2,128)S(1)}, f32[160,2]{0,1:T(2,128)}, u32[]{:S(2)}) copy-start(f32[160,2]{0,1:T(2,128)} %param.12) | copy-start | bytes 3844
  91.1 5.7 %copy-start.5 = (f32[160]{0:T(256)S(1)}, f32[160]{0:T(256)}, u32[]{:S(2)}) copy-start(f32[160]{0:T(256)} %param.11) | copy-start | bytes 1924
  91.2 54.4 %all-to-all-start.1 = ((bf16[8,60,2048]{2,1,0:T(8,128)(2,1)}), bf16[8,60,2048]{2,1,0:T(8,128)(2,1)}, u32[]{:S(2)}, u32[]{:S(2)}) async-start(bf16[8,60,2048]{2,1,0:T(8,128)(2,1)} %reshape_transpose_reshape.4), calls=%async_computation.1 | async-start | bytes 4194304 | tf_op jit(solution)/shard_map/all_to_all | solution.py:53
  153.4 4.1 %copy-start = (bf16[160,2048]{1,0:T(8,128)(2,1)S(1)}, bf16[160,2048]{1,0:T(8,128)(2,1)}, u32[]{:S(2)}) copy-start(bf16[160,2048]{1,0:T(8,128)(2,1)} %param.9) | copy-start | bytes 1966084
  157.5 0.7 copy-start.2
  157.5 0.7 copy-start.3
Sparse Core Ops, SparseCore 0:
  8.9 25.2 all-gather.3
  35.8 22.5 all-gather.5
  60.0 22.5 all-gather.7
where the time goes:
time: 166 us
  waiting for transfers between devices  102 us (61%)
  local copies, waits for them, and re-layouts  20.8 us (13%)
  between operations  13.3 us (8%)
  starting transfers between devices  13 us (8%)
  matrix products  9.41 us (6%)
  other arithmetic  7.63 us (5%)
    all_to_all x1, waiting for transfers between devices, body(): lax.all_to_all(results, 'ep', split_axis=0, concat_axis=0, tiled=True)  48.6 us
    all_to_all x1, waiting for transfers between devices, body(): lax.all_to_all(send_buf, 'ep', split_axis=0, concat_axis=0, tiled=True)  47.5 us
    all_to_all x1, starting transfers between devices, body(): lax.all_to_all(send_buf, 'ep', split_axis=0, concat_axis=0, tiled=True)  7.28 us
    dot_general x1, matrix products, body(): jnp.einsum('lrf,lfd->lrd', hidden, down_piece, preferred_element_type=jnp...  5.85 us
    all_to_all x1, starting transfers between devices, body(): lax.all_to_all(results, 'ep', split_axis=0, concat_axis=0, tiled=True)  5.64 us
    reduce_sum x1, other arithmetic, body(): jnp.sum(route_weight[:, :, None] * picked.astype(jnp.float32), axis=1)  4.05 us
    all_gather x1, waiting for transfers between devices, body(): down_piece = lax.all_gather(down_w, 'tp', axis=1, tiled=True)  3.67 us
    dot_general x1, matrix products, body(): jnp.einsum('lrd,lfd->lrf', expert_rows, gate_piece, preferred_element_typ...  3.56 us
  transfers between devices with their start and end apart: 5, of which 3 were waited for; matrix products, arithmetic and copies ran while one was open for 9% of the time, Pallas kernels for 0%

commit v1 on v0

--- a/solution.py
+++ b/solution.py
@@ -1,6 +1,10 @@
+import functools
+
 import jax
 import jax.numpy as jnp
 from jax import lax
+from jax.experimental import pallas as pl
+from jax.experimental.pallas import tpu as pltpu
 from jax.sharding import PartitionSpec as P
 
 TOP = 2
@@ -60,7 +64,272 @@
     return layer_norm(residual, out_gain, out_shift)
 
 
+MESH = pl.DeviceIdType.MESH
+CHUNKS = 4
+
+
+def cdot(a, b):
+    return jnp.dot(a, b, preferred_element_type=jnp.float32)
+
+
+def ndot(a, b, precision=None):
+    return lax.dot_general(
+        a, b, (((1,), (1,)), ((), ())), precision=precision, preferred_element_type=jnp.float32
+    )
+
+
+def fused(
+    half, cap, ids_ref, group_ref, share_ref, tok_ref, gate_ref, up_ref, down_ref, gain_ref,
+    shift_ref, out_ref, meta, mmeta, mtok, send_own, send_mir, recv_own, recv_mir, wgu, wd,
+    hid_own, hid_mir, res_own, res_mir, ret_own, ret_mir, part, mpart, total, send_sem, recv_sem,
+):
+    rows, width = tok_ref.shape
+    fpart = gate_ref.shape[0]
+    fc = width // CHUNKS
+    ep, tp = lax.axis_index("ep"), lax.axis_index("tp")
+    lo = lax.rem(ep, half)
+    base = ep - lo
+    mirror = {"ep": lax.rem(ep + half, 2 * half)}
+    pair = {"tp": tp + 1 - 2 * lax.rem(tp, 2)}
+    across = {"tp": lax.rem(tp + 2, 4)}
+    ahead = [{"ep": base + lax.rem(lo + r, half)} for r in range(half)]
+    behind = [{"ep": base + lax.rem(lo + half - r, half)} for r in range(half)]
+
+    barrier = pltpu.get_barrier_semaphore()
+    peers = [mirror, pair, across] + ahead[1:]
+    for peer in peers:
+        pl.semaphore_signal(barrier, inc=1, device_id=peer, device_id_type=MESH)
+    pl.semaphore_wait(barrier, len(peers))
+
+    started = []
+
+    def send(src, dst, peer):
+        i = len(started)
+        copy = pltpu.make_async_remote_copy(
+            src_ref=src, dst_ref=dst, send_sem=send_sem.at[i], recv_sem=recv_sem.at[i],
+            device_id=peer, device_id_type=MESH,
+        )
+        copy.start()
+        started.append(copy)
+        return copy
+
+    def cols(c):
+        return pl.ds(c * fc, fc)
+
+    def block(r):
+        return pl.ds(r * cap, cap)
+
+    meta[...] = jnp.zeros_like(meta)
+    share = share_ref[...]
+    weight = group_ref[...] * (share / jnp.sum(share, axis=0, keepdims=True))
+    meta[0:2, 0:rows] = ids_ref[...].astype(jnp.float32)
+    meta[2:4, 0:rows] = weight
+    tok_in = [send(tok_ref.at[:, cols(0)], mtok.at[:, cols(0)], mirror)]
+    gate_rows, up_rows = pl.ds(0, fpart), pl.ds(fpart, fpart)
+
+    def wrows(s):
+        return pl.ds(s * fpart, fpart)
+
+    gate2 = send(gate_ref, wgu.at[2, gate_rows], across)
+    up2 = send(up_ref, wgu.at[2, up_rows], across)
+    down2 = send(down_ref, wd.at[wrows(2)], across)
+    gate1 = send(gate_ref, wgu.at[1, gate_rows], pair)
+    up1 = send(up_ref, wgu.at[1, up_rows], pair)
+    down1 = send(down_ref, wd.at[wrows(1)], pair)
+    meta_in = send(meta, mmeta, mirror)
+    for c in range(1, CHUNKS):
+        tok_in.append(send(tok_ref.at[:, cols(c)], mtok.at[:, cols(c)], mirror))
+    wgu[0, 0:fpart] = gate_ref[...]
+    wgu[0, fpart : 2 * fpart] = up_ref[...]
+    wd[0:fpart] = down_ref[...]
+
+    earlier = lax.broadcasted_iota(jnp.int32, (rows, rows), 0)
+    later = lax.broadcasted_iota(jnp.int32, (rows, rows), 1)
+    before = (earlier < later).astype(jnp.bfloat16)
+    same = (earlier == later).astype(jnp.float32)
+    names = (base + lax.rem(lo + lax.broadcasted_iota(jnp.int32, (8, rows), 0), half)).astype(
+        jnp.float32
+    )
+
+    def routing(table):
+        first, second = table[0:1, 0:rows] == names, table[1:2, 0:rows] == names
+        hits = jnp.where(first | second, 1.0, 0.0)
+        slots = cdot(hits.astype(jnp.bfloat16), before)
+        key = jnp.where(hits > 0.5, slots, -1.0)
+        value = jnp.where(first, table[2:3, 0:rows], 0.0) + jnp.where(
+            second, table[3:4, 0:rows], 0.0
+        )
+        place = lax.broadcasted_iota(jnp.int32, (cap, rows), 0).astype(jnp.float32)
+        pick = jnp.concatenate(
+            [jnp.where(place == key[r : r + 1], 1.0, 0.0) for r in range(half)], axis=0
+        ).astype(jnp.bfloat16)
+        key_col = ndot(same, key, lax.Precision.HIGHEST)
+        value_col = ndot(same, value, lax.Precision.HIGHEST)
+        lane = lax.broadcasted_iota(jnp.int32, (rows, half * cap), 1)
+        merge = jnp.zeros((rows, half * cap), jnp.float32)
+        for r in range(half):
+            at = (lane - r * cap).astype(jnp.float32) == key_col[:, r : r + 1]
+            at = at & (lane >= r * cap)
+            merge = jnp.where(at, value_col[:, r : r + 1], merge)
+        high = merge.astype(jnp.bfloat16)
+        low = (merge - high.astype(jnp.float32)).astype(jnp.bfloat16)
+        return pick, high, low
+
+    def pack(pick, source, send_buf, recv_buf, c):
+        packed = cdot(pick, source[:, cols(c)]).astype(jnp.bfloat16)
+        recv_buf[block(0), cols(c)] = packed[0:cap]
+        send_buf[:, cols(c)] = packed
+        return [
+            send(send_buf.at[block(r), cols(c)], recv_buf.at[block(r), cols(c)], ahead[r])
+            for r in range(1, half)
+        ]
+
+    pick, high_own, low_own = routing(meta)
+    own_in = []
+    for c in range(CHUNKS):
+        own_in += pack(pick, tok_ref, send_own, recv_own, c)
+
+    def gate_up(s, recv_buf, hid):
+        both = ndot(recv_buf[...], wgu[s])
+        gate, up = both[:, 0:fpart], both[:, fpart : 2 * fpart]
+        hid[:, wrows(s)] = (gate / (1.0 + jnp.exp(-gate)) * up).astype(jnp.bfloat16)
+
+    meta_in.wait_recv()
+    pick, high_mir, low_mir = routing(mmeta)
+    mir_in = []
+    tok_in[0].wait_recv()
+    mir_in += pack(pick, mtok, send_mir, recv_mir, 0)
+    gate2.wait_recv()
+    gate3 = send(wgu.at[2, gate_rows], wgu.at[3, gate_rows], pair)
+    tok_in[1].wait_recv()
+    mir_in += pack(pick, mtok, send_mir, recv_mir, 1)
+    for copy in own_in + [gate1, up1]:
+        copy.wait_recv()
+    gate_up(0, recv_own, hid_own)
+    gate_up(1, recv_own, hid_own)
+    tok_in[2].wait_recv()
+    mir_in += pack(pick, mtok, send_mir, recv_mir, 2)
+    up2.wait_recv()
+    up3 = send(wgu.at[2, up_rows], wgu.at[3, up_rows], pair)
+    gate_up(2, recv_own, hid_own)
+    tok_in[3].wait_recv()
+    mir_in += pack(pick, mtok, send_mir, recv_mir, 3)
+    gate3.wait_recv()
+    up3.wait_recv()
+    gate_up(3, recv_own, hid_own)
+    down2.wait_recv()
+    down3 = send(wd.at[wrows(2)], wd.at[wrows(3)], pair)
+    for copy in mir_in:
+        copy.wait_recv()
+    for s in range(4):
+        gate_up(s, recv_mir, hid_mir)
+    down1.wait_recv()
+    down3.wait_recv()
+
+    def project(hid, res, ret, c):
+        result = cdot(hid[...], wd[:, cols(c)]).astype(jnp.bfloat16)
+        ret[block(0), cols(c)] = result[0:cap]
+        res[:, cols(c)] = result
+        return [
+            send(res.at[block(r), cols(c)], ret.at[block(r), cols(c)], behind[r])
+            for r in range(1, half)
+        ]
+
+    def combine(high, low, ret, c):
+        return cdot(high, ret[:, cols(c)]) + cdot(low, ret[:, cols(c)])
+
+    back_mir = [project(hid_mir, res_mir, ret_mir, c) for c in range(CHUNKS)]
+    part_in = []
+    back_own = []
+    for c in range(CHUNKS):
+        for copy in back_mir[c]:
+            copy.wait_recv()
+        part[:, cols(c)] = combine(high_mir, low_mir, ret_mir, c).astype(jnp.bfloat16)
+        part_in.append(send(part.at[:, cols(c)], mpart.at[:, cols(c)], mirror))
+        back_own.append(project(hid_own, res_own, ret_own, c))
+
+    for c in range(CHUNKS):
+        for copy in back_own[c]:
+            copy.wait_recv()
+        total[:, cols(c)] = (
+            residual_scale * tok_ref[:, cols(c)].astype(jnp.float32)
+            + combine(high_own, low_own, ret_own, c)
+        )
+    mean = jnp.zeros((rows, 1), jnp.float32)
+    for c in range(CHUNKS):
+        part_in[c].wait_recv()
+        piece = total[:, cols(c)] + mpart[:, cols(c)].astype(jnp.float32)
+        total[:, cols(c)] = piece
+        mean = mean + jnp.sum(piece, axis=1, keepdims=True)
+    mean = mean / width
+    center = total[...] - mean
+    variance = jnp.sum(center * center, axis=1, keepdims=True) / width
+    out_ref[...] = (
+        center * lax.rsqrt(variance + norm_eps) * gain_ref[...] + shift_ref[...]
+    ).astype(jnp.bfloat16)
+    for copy in started:
+        copy.wait_send()
+
+
+def fast_body(
+    tokens, expert_ids, group_weight, expert_share, gate_w, up_w, down_w, out_gain, out_shift
+):
+    rows, width = tokens.shape
+    experts = lax.axis_size("ep")
+    half = experts // 2
+    fpart = gate_w.shape[1]
+    hidden = fpart * lax.axis_size("tp")
+    cap = -(-(3 * rows * TOP // (2 * experts)) // 16) * 16
+    lanes = -(-rows // 128) * 128
+    packed = half * cap
+    copies = 10 + CHUNKS * (2 + 4 * (half - 1))
+    bf = jnp.bfloat16
+    vmem = pl.BlockSpec(memory_space=pltpu.VMEM)
+    return pl.pallas_call(
+        functools.partial(fused, half, cap),
+        out_shape=jax.ShapeDtypeStruct((rows, width), bf),
+        in_specs=[vmem] * 9,
+        out_specs=vmem,
+        scratch_shapes=[
+            pltpu.VMEM((8, lanes), jnp.float32),
+            pltpu.VMEM((8, lanes), jnp.float32),
+            pltpu.VMEM((rows, width), bf),
+            pltpu.VMEM((packed, width), bf),
+            pltpu.VMEM((packed, width), bf),
+            pltpu.VMEM((packed, width), bf),
+            pltpu.VMEM((packed, width), bf),
+            pltpu.VMEM((4, 2 * fpart, width), bf),
+            pltpu.VMEM((hidden, width), bf),
+            pltpu.VMEM((packed, hidden), bf),
+            pltpu.VMEM((packed, hidden), bf),
+            pltpu.VMEM((packed, width), bf),
+            pltpu.VMEM((packed, width), bf),
+            pltpu.VMEM((packed, width), bf),
+            pltpu.VMEM((packed, width), bf),
+            pltpu.VMEM((rows, width), bf),
+            pltpu.VMEM((rows, width), bf),
+            pltpu.VMEM((rows, width), jnp.float32),
+            pltpu.SemaphoreType.DMA((copies,)),
+            pltpu.SemaphoreType.DMA((copies,)),
+        ],
+        compiler_params=pltpu.CompilerParams(
+            collective_id=0, has_side_effects=True, vmem_limit_bytes=56 * 1024 * 1024
+        ),
+    )(
+        expert_ids.T,
+        group_weight[None, :],
+        expert_share.T,
+        tokens,
+        gate_w[0],
+        up_w[0],
+        down_w[0],
+        out_gain[None, :],
+        out_shift[None, :],
+    )
+
+
 def solution(mesh):
+    paired = mesh.shape["tp"] == 4 and mesh.shape["ep"] % 2 == 0
     placed = (
         P(("ep", "tp"), None),
         P(("ep", "tp"), None),
@@ -73,5 +342,5 @@
         P(),
     )
     return jax.shard_map(
-        body, mesh=mesh, in_specs=placed, out_specs=P(("ep", "tp"), None), check_vma=False
-    )
+        fast_body if paired else body, mesh=mesh, in_specs=placed, out_specs=P(("ep", "tp"), None), check_vma=False
+    )

time: 166 us -> 89 us (0.54)
  waiting for transfers between devices: 102 us -> 0 us
  Pallas kernels: 0 us -> 86.8 us
  local copies, waits for them, and re-layouts: 20.8 us -> 1.98 us
  between operations: 13.3 us -> 0.01 us
  starting transfers between devices: 13 us -> 0 us
  matrix products: 9.41 us -> 0 us
  other arithmetic: 7.63 us -> 0 us
    all_to_all x2 -> x0, waiting for transfers between devices: 96.1 us -> none  [the longest x1 48.6 us: body(): lax.all_to_all(results, 'ep', split_axis=0, concat_axis=0, tiled=True)]
    pallas_call x0 -> x1, Pallas kernels: none -> 86.8 us  [fast_body(): pl.pallas_call(functools.partial(fused, half, cap), out_shape=jax.ShapeDt...]
    all_to_all x2 -> x0, starting transfers between devices: 12.9 us -> none  [the longest x1 7.28 us: body(): lax.all_to_all(send_buf, 'ep', split_axis=0, concat_axis=0, tiled=True)]
    dot_general x2 -> x0, matrix products: 9.41 us -> none  [the longest x1 5.85 us: body(): jnp.einsum('lrf,lfd->lrd', hidden, down_piece, preferred_element_type=jnp...]
    reduce_sum x5 -> x0, other arithmetic: 4.71 us -> none  [the longest x1 4.05 us: body(): jnp.sum(route_weight[:, :, None] * picked.astype(jnp.float32), axis=1)]
    another operation x2 -> x0, local copies, waits for them, and re-layouts: 4.22 us -> none  [the longest x1 2.74 us: body(): results.transpose(1, 0, 2, 3)]
    reshape x3 -> x0, local copies, waits for them, and re-layouts: 3.83 us -> none  [the longest x1 1.74 us: body(): returned = returned.reshape(experts_all * capacity, model_width)]
    all_gather x3 -> x0, waiting for transfers between devices: 3.7 us -> none  [the longest x1 3.67 us: body(): down_piece = lax.all_gather(down_w, 'tp', axis=1, tiled=True)]
  transfers between devices with their start and end apart: 5 -> 0, of which waited for: 3 -> 0; matrix products, arithmetic and copies ran while one was open for 9% -> 0% of each run, Pallas kernels for 0% -> 0%
where the time goes in v1:
time: 89 us; the launch traced here: 88.8 us
  Pallas kernels  86.8 us (98%)
  local copies, waits for them, and re-layouts  1.98 us (2%)
    pallas_call x1, Pallas kernels, fast_body(): pl.pallas_call(functools.partial(fused, half, cap), out_shape=jax.ShapeDt...  86.8 us
    unnamed x1, local copies, waits for them, and re-layouts  1.98 us

profile of v1, /device:TPU:0, one launch (start us, length us, event | category | flops | bytes accessed | tf_op | source)
XLA Modules:
  0.0 88.8 jit_solution(8686038864987788475)
XLA Ops:
  0.0 86.8 %shard_map.91 = bf16[160,2048]{1,0:T(8,128)(2,1)} custom-call(s32[2,160]{1,0:T(2,128)} %bitcast.13, f32[1,160]{1,0:T(1,128)} %bitcast.15, f32[2,160]{1,0:T(2,128)} %bitcast.14, bf16[160,2048]{1,0:T(8,128)(2,1)} %tok_ref.1, bf16[128,2048]{1,0:T(8,128)(2,1)} %bitcast.8, bf16[128,2048]{1,0:T(8,128)(2,1)} %bitcast.9, bf16[128,2048]{1,0:T(8,128)(2,1)} %bitcast.10, ...), custom_call_target="tpu_custom_call" | custom-call | tf_op jit(solution)/shard_map/pallas_call | solution.py:288
  86.8 2.0 %copy.11 = bf16[160,2048]{1,0:T(8,128)(2,1)} copy(bf16[160,2048]{1,0:T(8,128)(2,1)} %shard_map.91) | data formatting | bytes 1310720

commit v2 on v1

--- a/solution.py
+++ b/solution.py
@@ -65,7 +65,8 @@
 
 
 MESH = pl.DeviceIdType.MESH
-CHUNKS = 4
+OUTWARD = (2, 2, 2, 1, 1)
+INWARD = (1, 1, 2, 2, 2)
 
 
 def cdot(a, b):
@@ -81,11 +82,15 @@
 def fused(
     half, cap, ids_ref, group_ref, share_ref, tok_ref, gate_ref, up_ref, down_ref, gain_ref,
     shift_ref, out_ref, meta, mmeta, mtok, send_own, send_mir, recv_own, recv_mir, wgu, wd,
-    hid_own, hid_mir, res_own, res_mir, ret_own, ret_mir, part, mpart, total, send_sem, recv_sem,
+    hid_own, hid_mir, res_own, res_mir, ret_own, ret_mir, part, mpart, total, acts, send_sem, recv_sem,
+    own_sem,
 ):
     rows, width = tok_ref.shape
     fpart = gate_ref.shape[0]
-    fc = width // CHUNKS
+    unit = width // 8
+    outward = [pl.ds(sum(OUTWARD[:c]) * unit, n * unit) for c, n in enumerate(OUTWARD)]
+    inward = [pl.ds(sum(INWARD[:c]) * unit, n * unit) for c, n in enumerate(INWARD)]
+    sides = [pl.ds(0, width // 2), pl.ds(width // 2, width // 2)]
     ep, tp = lax.axis_index("ep"), lax.axis_index("tp")
     lo = lax.rem(ep, half)
     base = ep - lo
@@ -113,9 +118,6 @@
         started.append(copy)
         return copy
 
-    def cols(c):
-        return pl.ds(c * fc, fc)
-
     def block(r):
         return pl.ds(r * cap, cap)
 
@@ -124,24 +126,36 @@
     weight = group_ref[...] * (share / jnp.sum(share, axis=0, keepdims=True))
     meta[0:2, 0:rows] = ids_ref[...].astype(jnp.float32)
     meta[2:4, 0:rows] = weight
-    tok_in = [send(tok_ref.at[:, cols(0)], mtok.at[:, cols(0)], mirror)]
     gate_rows, up_rows = pl.ds(0, fpart), pl.ds(fpart, fpart)
+    tok_in = []
+
+    def cross():
+        at = outward[len(tok_in)]
+        tok_in.append(send(tok_ref.at[:, at], mtok.at[:, at], mirror))
 
     def wrows(s):
         return pl.ds(s * fpart, fpart)
 
+    cross()
+    local = [
+        pltpu.make_async_copy(src, dst, own_sem.at[i])
+        for i, (src, dst) in enumerate(
+            [
+                (gate_ref, wgu.at[0, gate_rows]),
+                (up_ref, wgu.at[0, up_rows]),
+                (down_ref, wd.at[wrows(0)]),
+            ]
+        )
+    ]
+    for copy in local:
+        copy.start()
     gate2 = send(gate_ref, wgu.at[2, gate_rows], across)
     up2 = send(up_ref, wgu.at[2, up_rows], across)
-    down2 = send(down_ref, wd.at[wrows(2)], across)
+    down2 = [send(down_ref.at[:, side], wd.at[wrows(2), side], across) for side in sides]
     gate1 = send(gate_ref, wgu.at[1, gate_rows], pair)
     up1 = send(up_ref, wgu.at[1, up_rows], pair)
     down1 = send(down_ref, wd.at[wrows(1)], pair)
     meta_in = send(meta, mmeta, mirror)
-    for c in range(1, CHUNKS):
-        tok_in.append(send(tok_ref.at[:, cols(c)], mtok.at[:, cols(c)], mirror))
-    wgu[0, 0:fpart] = gate_ref[...]
-    wgu[0, fpart : 2 * fpart] = up_ref[...]
-    wd[0:fpart] = down_ref[...]
 
     earlier = lax.broadcasted_iota(jnp.int32, (rows, rows), 0)
     later = lax.broadcasted_iota(jnp.int32, (rows, rows), 1)
@@ -175,91 +189,120 @@
         low = (merge - high.astype(jnp.float32)).astype(jnp.bfloat16)
         return pick, high, low
 
-    def pack(pick, source, send_buf, recv_buf, c):
-        packed = cdot(pick, source[:, cols(c)]).astype(jnp.bfloat16)
-        recv_buf[block(0), cols(c)] = packed[0:cap]
-        send_buf[:, cols(c)] = packed
+    def pack(pick, source, send_buf, recv_buf, at):
+        packed = cdot(pick, source[:, at]).astype(jnp.bfloat16)
+        recv_buf[block(0), at] = packed[0:cap]
+        send_buf[:, at] = packed
+
+    def scatter(send_buf, recv_buf, at, peers):
         return [
-            send(send_buf.at[block(r), cols(c)], recv_buf.at[block(r), cols(c)], ahead[r])
+            send(send_buf.at[block(r), at], recv_buf.at[block(r), at], peers[r])
             for r in range(1, half)
         ]
 
-    pick, high_own, low_own = routing(meta)
-    own_in = []
-    for c in range(CHUNKS):
-        own_in += pack(pick, tok_ref, send_own, recv_own, c)
-
-    def gate_up(s, recv_buf, hid):
-        both = ndot(recv_buf[...], wgu[s])
+    def pack_mirrored():
+        c = len(mir_in)
+        tok_in[c].wait_recv()
+        pack(pick_mir, mtok, send_mir, recv_mir, outward[c])
+        mir_in.append(scatter(send_mir, recv_mir, outward[c], ahead))
+
+    def arrived(copies):
+        for copy in copies:
+            copy.wait_recv()
+
+    def activate(both):
         gate, up = both[:, 0:fpart], both[:, fpart : 2 * fpart]
-        hid[:, wrows(s)] = (gate / (1.0 + jnp.exp(-gate)) * up).astype(jnp.bfloat16)
-
+        return (gate / (1.0 + jnp.exp(-gate)) * up).astype(jnp.bfloat16)
+
+    def gate_up(s):
+        hid_own[:, wrows(s)] = activate(ndot(recv_own[...], wgu[s]))
+
+    pick_own, high_own, low_own = routing(meta)
+    for side in sides:
+        pack(pick_own, tok_ref, send_own, recv_own, side)
+    cross()
+    own_in = scatter(send_own, recv_own, pl.ds(0, width), ahead)
+    cross()
+    cross()
+    cross()
+    mir_in = []
     meta_in.wait_recv()
-    pick, high_mir, low_mir = routing(mmeta)
-    mir_in = []
-    tok_in[0].wait_recv()
-    mir_in += pack(pick, mtok, send_mir, recv_mir, 0)
+    pick_mir, high_mir, low_mir = routing(mmeta)
+    pack_mirrored()
     gate2.wait_recv()
     gate3 = send(wgu.at[2, gate_rows], wgu.at[3, gate_rows], pair)
-    tok_in[1].wait_recv()
-    mir_in += pack(pick, mtok, send_mir, recv_mir, 1)
-    for copy in own_in + [gate1, up1]:
-        copy.wait_recv()
-    gate_up(0, recv_own, hid_own)
-    gate_up(1, recv_own, hid_own)
-    tok_in[2].wait_recv()
-    mir_in += pack(pick, mtok, send_mir, recv_mir, 2)
+    pack_mirrored()
+    arrived(own_in + [gate1, up1])
+    for copy in local:
+        copy.wait()
+    gate_up(0)
+    gate_up(1)
+    pack_mirrored()
     up2.wait_recv()
     up3 = send(wgu.at[2, up_rows], wgu.at[3, up_rows], pair)
-    gate_up(2, recv_own, hid_own)
-    tok_in[3].wait_recv()
-    mir_in += pack(pick, mtok, send_mir, recv_mir, 3)
-    gate3.wait_recv()
-    up3.wait_recv()
-    gate_up(3, recv_own, hid_own)
-    down2.wait_recv()
-    down3 = send(wd.at[wrows(2)], wd.at[wrows(3)], pair)
-    for copy in mir_in:
+    gate_up(2)
+    pack_mirrored()
+    arrived([gate3, up3])
+    gate_up(3)
+    down2[0].wait_recv()
+    down3 = [send(wd.at[wrows(2), sides[0]], wd.at[wrows(3), sides[0]], pair)]
+    pack_mirrored()
+
+    main = width - OUTWARD[-1] * unit
+    for copies in mir_in[:-1]:
+        arrived(copies)
+    for s in range(4):
+        acts[s] = ndot(recv_mir[:, 0:main], wgu[s, :, 0:main])
+
+    def project(hid, res, ret, at):
+        result = cdot(hid[...], wd[:, at]).astype(jnp.bfloat16)
+        ret[block(0), at] = result[0:cap]
+        res[:, at] = result
+        return scatter(res, ret, at, behind)
+
+    def combine(high, low, ret, at):
+        return cdot(high, ret[:, at]) + cdot(low, ret[:, at])
+
+    arrived([down1, down3[0]])
+    arrived(mir_in[-1])
+    for s in range(4):
+        hid_mir[:, wrows(s)] = activate(
+            acts[s] + ndot(recv_mir[:, main:width], wgu[s, :, main:width])
+        )
+    back_mir = [project(hid_mir, res_mir, ret_mir, inward[0])]
+    back_mir.append(project(hid_mir, res_mir, ret_mir, inward[1]))
+    part_in = []
+
+    def give_back():
+        c = len(part_in)
+        at = inward[c]
+        arrived(back_mir[c])
+        part[:, at] = combine(high_mir, low_mir, ret_mir, at).astype(jnp.bfloat16)
+        part_in.append(send(part.at[:, at], mpart.at[:, at], mirror))
+
+    back_mir.append(project(hid_mir, res_mir, ret_mir, inward[2]))
+    give_back()
+    back_own = project(hid_own, res_own, ret_own, sides[0])
+    give_back()
+    down2[1].wait_recv()
+    down3.append(send(wd.at[wrows(2), sides[1]], wd.at[wrows(3), sides[1]], pair))
+    give_back()
+    down3[1].wait_recv()
+    back_mir.append(project(hid_mir, res_mir, ret_mir, inward[3]))
+    back_mir.append(project(hid_mir, res_mir, ret_mir, inward[4]))
+    back_own += project(hid_own, res_own, ret_own, sides[1])
+    give_back()
+    give_back()
+    arrived(back_own)
+    for at in inward:
+        total[:, at] = residual_scale * tok_ref[:, at].astype(jnp.float32) + combine(
+            high_own, low_own, ret_own, at
+        )
+    mean = jnp.zeros((rows, 1), jnp.float32)
+    for copy, at in zip(part_in, inward):
         copy.wait_recv()
-    for s in range(4):
-        gate_up(s, recv_mir, hid_mir)
-    down1.wait_recv()
-    down3.wait_recv()
-
-    def project(hid, res, ret, c):
-        result = cdot(hid[...], wd[:, cols(c)]).astype(jnp.bfloat16)
-        ret[block(0), cols(c)] = result[0:cap]
-        res[:, cols(c)] = result
-        return [
-            send(res.at[block(r), cols(c)], ret.at[block(r), cols(c)], behind[r])
-            for r in range(1, half)
-        ]
-
-    def combine(high, low, ret, c):
-        return cdot(high, ret[:, cols(c)]) + cdot(low, ret[:, cols(c)])
-
-    back_mir = [project(hid_mir, res_mir, ret_mir, c) for c in range(CHUNKS)]
-    part_in = []
-    back_own = []
-    for c in range(CHUNKS):
-        for copy in back_mir[c]:
-            copy.wait_recv()
-        part[:, cols(c)] = combine(high_mir, low_mir, ret_mir, c).astype(jnp.bfloat16)
-        part_in.append(send(part.at[:, cols(c)], mpart.at[:, cols(c)], mirror))
-        back_own.append(project(hid_own, res_own, ret_own, c))
-
-    for c in range(CHUNKS):
-        for copy in back_own[c]:
-            copy.wait_recv()
-        total[:, cols(c)] = (
-            residual_scale * tok_ref[:, cols(c)].astype(jnp.float32)
-            + combine(high_own, low_own, ret_own, c)
-        )
-    mean = jnp.zeros((rows, 1), jnp.float32)
-    for c in range(CHUNKS):
-        part_in[c].wait_recv()
-        piece = total[:, cols(c)] + mpart[:, cols(c)].astype(jnp.float32)
-        total[:, cols(c)] = piece
+        piece = total[:, at] + mpart[:, at].astype(jnp.float32)
+        total[:, at] = piece
         mean = mean + jnp.sum(piece, axis=1, keepdims=True)
     mean = mean / width
     center = total[...] - mean
@@ -282,13 +325,14 @@
     cap = -(-(3 * rows * TOP // (2 * experts)) // 16) * 16
     lanes = -(-rows // 128) * 128
     packed = half * cap
-    copies = 10 + CHUNKS * (2 + 4 * (half - 1))
+    parts = len(OUTWARD) + len(INWARD)
+    copies = 12 + parts + (half - 1) * (parts + 3)
     bf = jnp.bfloat16
     vmem = pl.BlockSpec(memory_space=pltpu.VMEM)
     return pl.pallas_call(
         functools.partial(fused, half, cap),
         out_shape=jax.ShapeDtypeStruct((rows, width), bf),
-        in_specs=[vmem] * 9,
+        in_specs=[vmem] * 4 + [pl.BlockSpec(memory_space=pl.ANY)] * 3 + [vmem] * 2,
         out_specs=vmem,
         scratch_shapes=[
             pltpu.VMEM((8, lanes), jnp.float32),
@@ -309,8 +353,10 @@
             pltpu.VMEM((rows, width), bf),
             pltpu.VMEM((rows, width), bf),
             pltpu.VMEM((rows, width), jnp.float32),
+            pltpu.VMEM((4, packed, 2 * fpart), jnp.float32),
             pltpu.SemaphoreType.DMA((copies,)),
             pltpu.SemaphoreType.DMA((copies,)),
+            pltpu.SemaphoreType.DMA((3,)),
         ],
         compiler_params=pltpu.CompilerParams(
             collective_id=0, has_side_effects=True, vmem_limit_bytes=56 * 1024 * 1024

time: 89 us -> 87.8 us (0.987)
  Pallas kernels: 86.8 us -> 85.7 us
    pallas_call x1, Pallas kernels: 86.8 us -> 85.7 us  [fast_body(): pl.pallas_call(functools.partial(fused, half, cap), out_shape=jax.ShapeDt...]
where the time goes in v2:
time: 87.8 us; the launch traced here: 87.7 us
  Pallas kernels  85.7 us (98%)
  local copies, waits for them, and re-layouts  1.98 us (2%)
    pallas_call x1, Pallas kernels, fast_body(): pl.pallas_call(functools.partial(fused, half, cap), out_shape=jax.ShapeDt...  85.7 us
    unnamed x1, local copies, waits for them, and re-layouts  1.98 us

profile of v2, /device:TPU:0, one launch (start us, length us, event | category | flops | bytes accessed | tf_op | source)
XLA Modules:
  0.0 87.7 jit_solution(12080047696943769013)
XLA Ops:
  0.0 85.7 %shard_map.91 = bf16[160,2048]{1,0:T(8,128)(2,1)} custom-call(s32[2,160]{1,0:T(2,128)} %bitcast.13, f32[1,160]{1,0:T(1,128)} %bitcast.15, f32[2,160]{1,0:T(2,128)} %bitcast.14, bf16[160,2048]{1,0:T(8,128)(2,1)} %tok_ref.1, bf16[128,2048]{1,0:T(8,128)(2,1)} %bitcast.8, bf16[128,2048]{1,0:T(8,128)(2,1)} %bitcast.9, bf16[128,2048]{1,0:T(8,128)(2,1)} %bitcast.10, ...), custom_call_target="tpu_custom_call" | custom-call | tf_op jit(solution)/shard_map/pallas_call | solution.py:332
  85.7 2.0 %copy.11 = bf16[160,2048]{1,0:T(8,128)(2,1)} copy(bf16[160,2048]{1,0:T(8,128)(2,1)} %shard_map.91) | data formatting | bytes 1310720
